TPU v7x, 32 devices: a whole 2x2x4 slice. The times are simulated.
32 devices in a mesh: rep: 2 (over x), fs: 8 (over z, y), tp: 2 (over core).
Axes of the slice: x: 2, y: 2, z: 4, core: 2. Of those that a mesh axis runs over, the one named last changes fastest.
Arguments:
- tokens: bfloat16 [4096, 2048], P(('rep', 'fs')), may hold values from -6 to 6
- first_gain: float32 [2048], replicated, may hold values from 0.1 to 1.9
- value_weight: float32 [2048, 1024], P('fs', 'tp'), may hold values from -0.125 to 0.125
- gate_weight: float32 [2048, 1024], P('fs', 'tp'), may hold values from -0.125 to 0.125
- value_scale: float32 [1024], P('tp'), may hold values from 0.5 to 2
- gate_scale: float32 [1024], P('tp'), may hold values from 0.5 to 2
- conv_taps: float32 [31, 1024], P(None, 'tp'), may hold values from -7 to 7
- chan_gain: float32 [1024], P('tp'), may hold values from 0.1 to 1.9
- mixout_weight: float32 [1024, 2048], P('tp', 'fs'), may hold values from -0.1875 to 0.1875
- mixout_scale: float32 [2048], P('fs'), may hold values from 0.5 to 2
- second_gain: float32 [2048], replicated, may hold values from 0.1 to 1.9
- up_weight: float32 [2048, 8192], P('fs', 'tp'), may hold values from -0.125 to 0.125
- up_scale: float32 [8192], P('tp'), may hold values from 0.5 to 2
- down_weight: float32 [8192, 2048], P('tp', 'fs'), may hold values from -0.0625 to 0.0625
- down_scale: float32 [2048], P('fs'), may hold values from 0.5 to 2
Outputs:
- layer_out: bfloat16 [4096, 2048], P(('rep', 'fs'))
All inputs are finite; a program needn't handle non-finite values.
Results may differ from a plain program's by a relative error of at most 0.025.
Values may be sent and summed in bfloat16 or wider, within the bound.
A program may use at most 128 MiB of HBM per device.

v0:
```python
import functools

import jax
import jax.numpy as jnp
import numpy as np
from jax import lax
from jax.experimental import pallas as pl
from jax.experimental.pallas import tpu as pltpu
from jax.sharding import PartitionSpec as P

SEQ_LEN = 128


def rms_rows(rows, gain):
    values = rows.astype(jnp.float32)
    scaled = values * lax.rsqrt(jnp.mean(values * values, axis=-1, keepdims=True) + 1e-05)
    return (scaled * gain).astype(jnp.bfloat16)


def causal_conv(signal, taps):
    width = signal.shape[1]
    seqs = signal.reshape(-1, SEQ_LEN, width)
    result = lax.conv_general_dilated(
        seqs,
        taps[:, None, :],
        (1,),
        [(taps.shape[0] - 1, 0)],
        dimension_numbers=("NWC", "WIO", "NWC"),
        feature_group_count=width,
        precision=lax.Precision.HIGHEST,
    )
    return result.reshape(signal.shape)


def on_device(
    tokens,
    first_gain,
    value_weight,
    gate_weight,
    value_scale,
    gate_scale,
    conv_taps,
    chan_gain,
    mixout_weight,
    mixout_scale,
    second_gain,
    up_weight,
    up_scale,
    down_weight,
    down_scale,
):
    normed = rms_rows(tokens, first_gain)
    count = normed.shape[0]
    width = value_weight.shape[1]
    columns = normed
    value_sum = jnp.dot(
        columns,
        lax.all_gather(value_weight.astype(jnp.bfloat16), "fs", axis=0, tiled=True),
        preferred_element_type=jnp.float32,
    )
    gate_sum = jnp.dot(
        columns,
        lax.all_gather(gate_weight.astype(jnp.bfloat16), "fs", axis=0, tiled=True),
        preferred_element_type=jnp.float32,
    )
    value_mult = value_scale.astype(jnp.bfloat16).astype(jnp.float32)
    gate_mult = gate_scale.astype(jnp.bfloat16).astype(jnp.float32)
    glu = value_sum * value_mult * jax.nn.sigmoid(gate_sum * gate_mult)
    conv = causal_conv(glu, conv_taps)
    total = width * lax.axis_size("tp")
    sums, squares = lax.psum((jnp.sum(conv, axis=1), jnp.sum(conv * conv, axis=1)), "tp")
    mean = sums / total
    var = squares / total - mean * mean
    centred = conv - mean[:, None]
    mixed_in = jax.nn.silu(centred * lax.rsqrt(var[:, None] + 1e-05) * chan_gain).astype(
        jnp.bfloat16
    )
    out_whole, out_mult = (
        lax.all_gather(mixout_weight.astype(jnp.bfloat16), "fs", axis=1, tiled=True),
        lax.all_gather(mixout_scale.astype(jnp.bfloat16), "fs", axis=0, tiled=True),
    )
    out_factor = out_mult.astype(jnp.float32)
    mix_term = jnp.dot(mixed_in, out_whole, preferred_element_type=jnp.float32) * out_factor
    mix_sum = lax.psum(mix_term.astype(jnp.bfloat16), "tp").astype(jnp.float32)
    middle = (tokens.astype(jnp.float32) + mix_sum).astype(jnp.bfloat16)
    normed2 = rms_rows(middle, second_gain)
    up_empty = jnp.zeros((count, up_weight.shape[1]), jnp.float32)
    piece = lax.all_gather(up_weight.astype(jnp.bfloat16), "fs", axis=0, tiled=True)
    columns = lax.slice_in_dim(normed2, 0, piece.shape[0], axis=1)
    up_sum = up_empty + jnp.dot(columns, piece, preferred_element_type=jnp.float32)
    up_mult = up_scale.astype(jnp.bfloat16).astype(jnp.float32)
    hidden = jnp.square(jax.nn.relu(up_sum * up_mult)).astype(jnp.bfloat16)
    down_whole, down_mult = (
        lax.all_gather(down_weight.astype(jnp.bfloat16), "fs", axis=1, tiled=True),
        lax.all_gather(down_scale.astype(jnp.bfloat16), "fs", axis=0, tiled=True),
    )
    down_factor = down_mult.astype(jnp.float32)
    down_term = jnp.dot(hidden, down_whole, preferred_element_type=jnp.float32) * down_factor
    down_sum = lax.psum(down_term.astype(jnp.bfloat16), "tp").astype(jnp.float32)
    return (middle.astype(jnp.float32) + down_sum).astype(jnp.bfloat16)


def ring_order(mesh):
    axis = mesh.axis_names.index("fs")
    line = np.moveaxis(mesh.devices, axis, 0).reshape(mesh.shape["fs"], -1)[:, 0]
    places = [getattr(d, "coords", None) for d in line]
    if any(p is None for p in places):
        return list(range(len(places)))
    at = {(p[2], p[1]): i for i, p in enumerate(places)}
    zs, ys = sorted({k[0] for k in at}), sorted({k[1] for k in at})
    if len(at) != len(zs) * len(ys) or len(zs) % 2 or len(ys) < 2:
        return list(range(len(places)))
    order = []
    for row, z in enumerate(zs):
        order += [at[z, y] for y in (ys[1:] if row % 2 == 0 else ys[:0:-1])]
    return order + [at[z, ys[0]] for z in reversed(zs)]


MESH = pl.DeviceIdType.MESH
F32, B16 = jnp.float32, jnp.bfloat16


def pick(table, index):
    value = jnp.int32(table[0])
    for i in range(1, len(table)):
        value = jnp.where(index == i, jnp.int32(table[i]), value)
    return value


def remote(src, dst, send_sem, recv_sem, target):
    return pltpu.make_async_remote_copy(
        src_ref=src,
        dst_ref=dst,
        send_sem=send_sem,
        recv_sem=recv_sem,
        device_id=target,
        device_id_type=MESH,
    )


def greet(targets):
    barrier = pltpu.get_barrier_semaphore()
    for target in targets:
        pl.semaphore_signal(barrier, inc=1, device_id=target, device_id_type=MESH)
    pl.semaphore_wait(barrier, len(targets))


def ring_targets(order):
    n = len(order)
    here = lax.axis_index("fs")
    up = pick([order[(order.index(i) + 1) % n] for i in range(n)], here)
    down = pick([order[(order.index(i) - 1) % n] for i in range(n)], here)
    return {"fs": up}, {"fs": down}


def ring_round(n, block, half, sems, up, down, landed=None):
    send, recv = sems
    middle = n // 2
    started = []
    for step in range(1, middle + 1):
        pair = []
        if step < middle:
            low_from, high_from = block((n - step + 1) % n), block(step - 1)
            low_to, high_to = block(n - step), block(step)
        else:
            low_from, high_from = half((n - step + 1) % n, 0), half(step - 1, 1)
            low_to, high_to = half(middle, 0), half(middle, 1)
        low_sem, high_sem = n - step, (step if step < middle else n)
        pair.append(remote(low_from, low_to, send.at[low_sem], recv.at[low_sem], up))
        pair.append(remote(high_from, high_to, send.at[high_sem], recv.at[high_sem], down))
        for copy in pair:
            copy.start()
        started += pair
        yield
        for copy in pair:
            copy.wait_recv()
        if landed is not None:
            for k in [n - step, step] if step < middle else [middle]:
                landed(k)
    for copy in started:
        copy.wait_send()


def run_together(rounds):
    live = list(rounds)
    while live:
        for one in list(live):
            try:
                next(one)
            except StopIteration:
                live.remove(one)


def weights_kernel(order, mine, other, piece, cut, rest, mine_all, other_all, piece_all, own_flat, rest_flat,
                   ring_send, ring_recv, out_send, out_recv, x_send, x_recv, cut_send, cut_recv, swap_send, swap_recv, local):
    n = len(order)
    here, rep = lax.axis_index("fs"), lax.axis_index("rep")
    up, down = ring_targets(order)
    partner = {"rep": 1 - rep}
    peers = [{"fs": lax.rem(here + k, n)} for k in range(1, n)]
    greet(peers + [partner])
    rows, cols = mine.shape[0], piece.shape[1]

    def first(k):
        return mine if k == 0 else mine_all.at[pl.ds(k * rows, rows)]

    def first_half(k, i):
        size = rows // 2
        if k == 0:
            return mine.at[pl.ds(i * size, size)]
        return mine_all.at[pl.ds(k * rows + i * size, size)]

    def second(k):
        return piece if k == 0 else piece_all.at[:, pl.ds(k * cols, cols)]

    def second_half(k, i):
        size = piece.shape[0] // 2
        if k == 0:
            return piece.at[pl.ds(i * size, size)]
        return piece_all.at[pl.ds(i * size, size), pl.ds(k * cols, cols)]

    crossing = []

    def landed(k):
        there = pl.ds(k * rows, rows)
        copy = remote(mine_all.at[there], other_all.at[there], x_send.at[k], x_recv.at[k], partner)
        copy.start()
        crossing.append(copy)

    kept = [
        pltpu.make_async_copy(mine, mine_all.at[pl.ds(0, rows)], local.at[0]),
        pltpu.make_async_copy(other, other_all.at[pl.ds(0, rows)], local.at[1]),
        pltpu.make_async_copy(piece, piece_all.at[:, pl.ds(0, cols)], local.at[2]),
        pltpu.make_async_copy(cut.at[here], own_flat.at[here], local.at[3]),
        pltpu.make_async_copy(rest, rest_flat.at[here], local.at[4]),
    ]
    for copy in kept:
        copy.start()
    run_together(
        [
            ring_round(n, first, first_half, (ring_send, ring_recv), up, down, landed),
            ring_round(n, second, second_half, (out_send, out_recv), up, down),
        ]
    )
    sends = []
    for k in range(1, n):
        to = lax.rem(here + k, n)
        copy = remote(cut.at[to], own_flat.at[here], cut_send.at[k], cut_recv.at[k], {"fs": to})
        copy.start()
        sends.append(copy)
    swaps = []
    for k in range(1, n):
        sends[k - 1].wait_recv()
        came = lax.rem(here - k + n, n)
        copy = remote(own_flat.at[came], rest_flat.at[came], swap_send.at[k], swap_recv.at[k], partner)
        copy.start()
        swaps.append(copy)
    for copy in sends:
        copy.wait_send()
    for copy in crossing + swaps:
        copy.wait()
    for copy in kept:
        copy.wait()


def tokens_kernel(order, rows_ref, ours, theirs, ring_send, ring_recv, tp_send, tp_recv, local):
    n = len(order)
    tp = lax.axis_index("tp")
    up, down = ring_targets(order)
    partner = {"tp": 1 - tp}
    greet([up, down, partner])
    count, wide = rows_ref.shape[0] // 2, rows_ref.shape[1]
    own = pl.ds(pl.multiple_of(tp * count, count), count)
    rest = pl.ds(pl.multiple_of((1 - tp) * count, count), count)

    def block(k):
        return rows_ref.at[own] if k == 0 else ours.at[pl.ds(k * count, count)]

    def half(k, i):
        size = wide // 2
        if k == 0:
            return rows_ref.at[own, pl.ds(i * size, size)]
        return ours.at[pl.ds(k * count, count), pl.ds(i * size, size)]

    crossing = []

    def landed(k):
        there = pl.ds(k * count, count)
        copy = remote(ours.at[there], theirs.at[there], tp_send.at[k], tp_recv.at[k], partner)
        copy.start()
        crossing.append(copy)

    kept = [
        pltpu.make_async_copy(rows_ref.at[own], ours.at[pl.ds(0, count)], local.at[0]),
        pltpu.make_async_copy(rows_ref.at[rest], theirs.at[pl.ds(0, count)], local.at[1]),
    ]
    for copy in kept:
        copy.start()
    run_together([ring_round(n, block, half, (ring_send, ring_recv), up, down, landed)])
    for copy in crossing + kept:
        copy.wait()


def sums_kernel(order, ours, theirs, middle, out, passed, going, coming, tp_send, tp_recv,
                ring_send, ring_recv, last):
    n = len(order)
    half_way = n // 2
    tp = lax.axis_index("tp")
    up, down = ring_targets(order)
    partner = {"tp": 1 - tp}
    greet([up, down, partner])
    count, wide = middle.shape[0] // 2, middle.shape[1]
    size = wide // 2
    needed = [half_way]
    for step in range(half_way - 1, 0, -1):
        needed += [step, n - step]
    needed.append(0)
    passing = {}
    for k in needed:
        there = pl.ds(k * count, count)
        passing[k] = remote(theirs.at[there], passed.at[there], tp_send.at[k], tp_recv.at[k], partner)
        passing[k].start()

    def part(k, cols=slice(None)):
        there = slice(k * count, (k + 1) * count)
        return ours[there, cols].astype(F32) + passed[there, cols].astype(F32)

    halves = (pl.ds(0, size), pl.ds(size, size))
    flights = []
    passing[half_way].wait_recv()
    far = part(half_way)
    for way, target in enumerate((up, down)):
        going[way, 0, :, way * size : (way + 1) * size] = far[:, way * size : (way + 1) * size].astype(B16)
        copy = remote(
            going.at[way, 0, :, halves[way]],
            coming.at[way, 0, :, halves[way]],
            ring_send.at[way, 0],
            ring_recv.at[way, 0],
            target,
        )
        copy.start()
        flights.append(copy)
    pair = flights[-2:]
    for hop, step in enumerate(range(half_way - 1, 0, -1), 1):
        fresh = []
        for way, target in enumerate((up, down)):
            k = step if way == 0 else n - step
            passing[k].wait_recv()
            pair[way].wait_recv()
            if hop == 1:
                near = slice(way * size, (way + 1) * size)
                other = slice((1 - way) * size, (2 - way) * size)
                going[way, hop, :, near] = (part(k, near) + coming[way, 0, :, near].astype(F32)).astype(B16)
                going[way, hop, :, other] = part(k, other).astype(B16)
            else:
                going[way, hop] = (part(k) + coming[way, hop - 1].astype(F32)).astype(B16)
            copy = remote(
                going.at[way, hop], coming.at[way, hop], ring_send.at[way, hop], ring_recv.at[way, hop], target
            )
            copy.start()
            fresh.append(copy)
        flights += fresh
        pair = fresh
    passing[0].wait_recv()
    for copy in pair:
        copy.wait_recv()
    hop = half_way - 1
    total = part(0) + coming[0, hop].astype(F32) + coming[1, hop].astype(F32)
    own = pl.ds(pl.multiple_of(tp * count, count), count)
    out[own, :] = (middle[own, :].astype(F32) + total).astype(B16)
    final = remote(out.at[own], out.at[own], last.at[0], last.at[1], partner)
    final.start()
    for copy in passing.values():
        copy.wait_send()
    for copy in flights:
        copy.wait_send()
    final.wait()


def call(kernel, outs, scratch, number, *operands):
    spec = pl.BlockSpec(memory_space=pltpu.VMEM)
    return pl.pallas_call(
        kernel,
        out_shape=[jax.ShapeDtypeStruct(shape, B16) for shape in outs],
        in_specs=[spec] * len(operands),
        out_specs=[spec] * len(outs),
        scratch_shapes=scratch,
        compiler_params=pltpu.CompilerParams(
            collective_id=number, has_side_effects=True, vmem_limit_bytes=56 * 1024 * 1024
        ),
    )(*operands)


def ring_device(order, *args):
    (
        tokens,
        first_gain,
        value_weight,
        gate_weight,
        value_scale,
        gate_scale,
        conv_taps,
        chan_gain,
        mixout_weight,
        mixout_scale,
        second_gain,
        up_weight,
        up_scale,
        down_weight,
        down_scale,
    ) = args
    f32, b16 = jnp.float32, jnp.bfloat16
    n = lax.axis_size("fs")
    here = lax.axis_index("fs")
    first_rep = lax.axis_index("rep") == 0
    place_of = [order.index(i) for i in range(n)]
    place = pick(place_of, here)

    def owner(offset):
        return pick(order, (place + offset) % n)

    def across(block, axis):
        return lax.ppermute(block, axis, [(0, 1), (1, 0)])

    mine = jnp.where(first_rep, value_weight, gate_weight).astype(b16)
    other = jnp.where(first_rep, gate_weight, value_weight).astype(b16)
    out_piece = (mixout_weight.astype(b16).astype(f32) * mixout_scale.astype(b16).astype(f32)).astype(b16)

    depth, wide = up_weight.shape[0], up_weight.shape[1] // n
    up_cut = jnp.stack([up_weight[:, k * wide : (k + 1) * wide] for k in range(n)])
    down_scaled = down_weight.astype(b16).astype(f32) * down_scale.astype(b16).astype(f32)
    down_cut = down_scaled.reshape(n, wide, down_weight.shape[1])
    down_cut = jnp.concatenate([down_cut[:, : wide // 2], down_cut[:, wide // 2 :]], axis=2)
    own_cut = jnp.where(first_rep, up_cut, down_cut).astype(b16)
    rest_cut = jnp.where(first_rep, down_cut, up_cut).astype(b16)
    here_rest = lax.dynamic_index_in_dim(rest_cut, here, 0, keepdims=False)
    rows, cols = mine.shape[0], out_piece.shape[1]
    dma = pltpu.SemaphoreType.DMA
    mine_all, other_all, out_all, own_flat, rest_flat = call(
        functools.partial(weights_kernel, order),
        [(n * rows, mine.shape[1])] * 2 + [(out_piece.shape[0], n * cols)] + [own_cut.shape] * 2,
        [dma((n + 1,))] * 4 + [dma((n,))] * 6 + [dma((5,))],
        0,
        mine,
        other,
        out_piece,
        own_cut,
        here_rest,
    )

    normed = rms_rows(tokens, first_gain)
    width = value_weight.shape[1]
    normed_turned = jnp.concatenate(
        [lax.dynamic_slice_in_dim(normed, owner(k) * depth, depth, axis=1) for k in range(n)], axis=1
    )
    mine_sum = jnp.dot(
        normed_turned, mine_all, preferred_element_type=f32
    )
    other_sum = jnp.dot(
        normed_turned, other_all, preferred_element_type=f32
    )

    value_sum = jnp.where(first_rep, mine_sum, other_sum)
    gate_sum = jnp.where(first_rep, other_sum, mine_sum)
    value_mult = value_scale.astype(b16).astype(f32)
    gate_mult = gate_scale.astype(b16).astype(f32)
    glu = value_sum * value_mult * jax.nn.sigmoid(gate_sum * gate_mult)
    conv = causal_conv(glu, conv_taps)
    total = width * lax.axis_size("tp")
    stats = jnp.stack([jnp.sum(conv, axis=1), jnp.sum(conv * conv, axis=1)])
    sums, squares = stats + across(stats, "tp")
    mean = sums / total
    var = squares / total - mean * mean
    centred = conv - mean[:, None]
    mixed_in = jax.nn.silu(centred * lax.rsqrt(var[:, None] + 1e-05) * chan_gain).astype(b16)
    mix_turned = jnp.dot(
        mixed_in, out_all, preferred_element_type=f32
    ).astype(b16)
    mix_term = jnp.concatenate(
        [
            lax.dynamic_slice_in_dim(mix_turned, (place_of[j] - place) % n * cols, cols, axis=1)
            for j in range(n)
        ],
        axis=1,
    )
    mix_sum = mix_term.astype(f32) + across(mix_term, "tp").astype(f32)
    middle = (tokens.astype(f32) + mix_sum).astype(b16)
    normed2 = rms_rows(middle, second_gain)

    count = normed2.shape[0] // 2
    ours, theirs = call(
        functools.partial(tokens_kernel, order),
        [(n * count, normed2.shape[1])] * 2,
        [dma((n + 1,))] * 2 + [dma((n,))] * 2 + [dma((2,))],
        1,
        normed2,
    )
    up_flat = jnp.where(first_rep, own_flat, rest_flat).reshape(n * depth, wide)
    down_flat = jnp.where(first_rep, rest_flat, own_flat)
    down_flat = jnp.concatenate(
        [jnp.concatenate([block[:, :cols], block[:, cols:]], axis=0) for block in down_flat], axis=1
    )
    mult = lax.dynamic_slice_in_dim(up_scale.astype(b16).astype(f32), here * wide, wide)

    def feed(rows):
        hidden = jnp.square(jax.nn.relu(jnp.dot(rows, up_flat, preferred_element_type=f32) * mult))
        return jnp.dot(hidden.astype(b16), down_flat, preferred_element_type=f32)

    half_way = n // 2
    full = (2, half_way, count, normed2.shape[1])
    (result,) = call(
        functools.partial(sums_kernel, order),
        [middle.shape],
        [
            pltpu.VMEM((n * count, normed2.shape[1]), b16),
            pltpu.VMEM(full, b16),
            pltpu.VMEM(full, b16),
            dma((n,)),
            dma((n,)),
            dma((2, half_way)),
            dma((2, half_way)),
            dma((2,)),
        ],
        2,
        feed(ours).astype(b16),
        feed(theirs).astype(b16),
        middle,
    )
    return result


def solution(mesh):
    placed = (
        P(("rep", "fs"), None),
        P(),
        P("fs", "tp"),
        P("fs", "tp"),
        P("tp"),
        P("tp"),
        P(None, "tp"),
        P("tp"),
        P("tp", "fs"),
        P("fs"),
        P(),
        P("fs", "tp"),
        P("tp"),
        P("tp", "fs"),
        P("fs"),
    )
    n = mesh.shape["fs"]
    small = mesh.shape["rep"] == 2 and mesh.shape["tp"] == 2 and n % 2 == 0 and 4 <= n <= 16
    body = functools.partial(ring_device, ring_order(mesh)) if small else on_device
    return jax.shard_map(
        body, mesh=mesh, in_specs=placed, out_specs=P(("rep", "fs"), None), check_vma=False
    )
```

profile of v0, /device:TPU:0, one launch (start us, length us, event | category | flops | bytes accessed | tf_op | source)
XLA Modules:
  0.0 294.6 jit_solution(2255014513948226049)
XLA Ops:
  1.4 1.5 fusion.5
  2.9 2.5 convert_multiply_fusion
  5.7 2.0 copy-done.5
  9.8 0.8 bitcast_dynamic-update-slice_fusion.4
  12.8 0.8 bitcast_dynamic-update-slice_fusion
  13.6 3.5 %fusion.1.cut = bf16[8,256,512]{2,1,0:T(8,128)(2,1)} fusion(bf16[8,256,512]{2,1,0:T(8,128)(2,1)} %bitcast_dynamic-update-slice_fusion, bf16[8,256,256]{2,1,0:T(8,128)(2,1)S(1)} %get-tuple-element.34, bf16[8,256,256]{2,1,0:T(8,128)(2,1)S(1)} %get-tuple-element.33, pred[]{:T(512)S(6)} %eq.209), kind=kLoop, calls=%fused_computation.4 | loop fusion | flops 5242880 | bytes 6291457 | tf_op jit(solution)/shard_map/convert_element_type | solution.py:434
  17.0 1.8 fusion.16.rest
  18.9 1.8 multiply_convert_fusion.3.piece
  20.7 2.1 select_convert_fusion
  23.4 111.6 %shard_map.145 = (bf16[2048,512]{1,0:T(8,128)(2,1)}, bf16[2048,512]{1,0:T(8,128)(2,1)}, bf16[512,2048]{1,0:T(8,128)(2,1)}, bf16[8,256,512]{2,1,0:T(8,128)(2,1)}, bf16[8,256,512]{2,1,0:T(8,128)(2,1)}) custom-call(bf16[256,512]{1,0:T(8,128)(2,1)} %get-tuple-element.36.mine, bf16[256,512]{1,0:T(8,128)(2,1)} %get-tuple-element.35.other, ...), custom_call_target="tpu_custom_call" | custom-call | tf_op jit(solution)/shard_map/pallas_call | solution.py:382
  135.1 2.4 fusion.33
  137.5 0.8 divide_multiply_fusion
  138.3 3.0 %fusion.22 = (f32[2,128]{0,1:T(8,128)S(1)}, f32[2,128]{0,1:T(8,128)S(1)}, f32[2,128,512]{2,0,1:T(2,128)}) fusion(f32[31,1,512]{2,0,1:T(8,128)S(1)} %bitcast.62, f32[2,128,512]{2,1,0:T(8,128)S(1)} %bitcast.73), kind=kOutput, calls=%fused_computation.96 | convolution fusion | flops 43437568 | bytes 1114112 | tf_op jit(solution)/shard_map/conv_general_dilated | solution.py:23
  141.7 3.2 %broadcast_select_fusion = (bf16[8,256,512]{2,1,0:T(8,128)(2,1)}, bf16[8,256,512]{2,1,0:T(8,128)(2,1)S(1)}) fusion(bf16[8,256,512]{2,1,0:T(8,128)(2,1)S(1)} %copy-done.4, bf16[8,256,512]{2,1,0:T(8,128)(2,1)} %get-tuple-element.17, pred[]{:T(512)S(6)} %eq.209), kind=kLoop, calls=%fused_computation.23 | loop fusion | flops 2097152 | bytes 8388609 | tf_op jit(solution)/shard_map/jit(_where)/select_n | solution.py:498
  147.4 0.8 maximum_dynamic-update-slice_fusion.4
  148.7 2.3 convolution_convert_fusion.2
  151.7 0.8 fusion.18
  153.2 0.8 maximum_dynamic-update-slice_fusion.2
  156.2 1.3 fusion.4.rows_ref
  157.5 59.8 %shard_map.146 = (bf16[1024,2048]{1,0:T(8,128)(2,1)}, bf16[1024,2048]{1,0:T(8,128)(2,1)}) custom-call(bf16[256,2048]{1,0:T(8,128)(2,1)} %fusion.4.rows_ref), custom_call_target="tpu_custom_call" | custom-call | tf_op jit(solution)/shard_map/pallas_call | solution.py:382
  217.3 9.9 %convolution_convert_fusion.1.ours = bf16[1024,2048]{1,0:T(8,128)(2,1)} fusion(bf16[512,2048]{1,0:T(8,128)(2,1)} %maximum_dynamic-update-slice_fusion, bf16[1024,2048]{1,0:T(8,128)(2,1)} %get-tuple-element.15, bf16[2048,512]{1,0:T(8,128)(2,1)} %bitcast.64, f32[512]{0:T(512)S(1)} %fusion.18), kind=kOutput, calls=%fused_computation.7 | convolution fusion | flops 4299161600 | bytes 12584960 | tf_op jit(solution)/shard_map/dot_general | solution.py:507
  227.2 9.9 %convolution_convert_fusion.theirs = bf16[1024,2048]{1,0:T(8,128)(2,1)} fusion(bf16[512,2048]{1,0:T(8,128)(2,1)} %maximum_dynamic-update-slice_fusion, bf16[1024,2048]{1,0:T(8,128)(2,1)} %get-tuple-element.18, bf16[2048,512]{1,0:T(8,128)(2,1)} %bitcast.65, f32[512]{0:T(512)S(1)} %fusion.18), kind=kOutput, calls=%fused_computation.6 | convolution fusion | flops 4299161600 | bytes 12584960 | tf_op jit(solution)/shard_map/dot_general | solution.py:507
  237.1 55.1 %shard_map.147 = bf16[256,2048]{1,0:T(8,128)(2,1)} custom-call(bf16[1024,2048]{1,0:T(8,128)(2,1)} %convolution_convert_fusion.1.ours, bf16[1024,2048]{1,0:T(8,128)(2,1)} %convolution_convert_fusion.theirs, bf16[256,2048]{1,0:T(8,128)(2,1)} %copy-done.3), custom_call_target="tpu_custom_call" | custom-call | tf_op jit(solution)/shard_map/pallas_call | solution.py:382
  292.3 2.3 copy.64
  (78 shorter events, 13.2 us)
Async XLA Ops:
  0.0 138.3 %copy-start = (f32[31,512]{1,0:T(8,128)S(1)}, f32[31,512]{1,0:T(8,128)}, u32[]{:S(2)}) copy-start(f32[31,512]{1,0:T(8,128)} %param.21) | copy-start | bytes 190468
  5.4 2.2 copy-start.5
  17.0 1.8 copy-start.10
  17.0 1.8 copy-start.11
  17.0 5.8 %copy-start.2 = (bf16[256,2048]{1,0:T(8,128)(2,1)S(1)}, bf16[256,2048]{1,0:T(8,128)(2,1)}, u32[]{:S(2)}) copy-start(bf16[256,2048]{1,0:T(8,128)(2,1)} %param.15) | copy-start | bytes 3145732
  17.0 5.8 %copy-start.7 = (f32[2048]{0:T(1024)S(1)}, f32[2048]{0:T(1024)}, u32[]{:S(2)}) copy-start(f32[2048]{0:T(1024)} %param.16) | copy-start | bytes 24580
  135.0 2.5 copy-start.12
  138.3 3.4 %copy-start.4 = (bf16[8,256,512]{2,1,0:T(8,128)(2,1)S(1)}, bf16[8,256,512]{2,1,0:T(8,128)(2,1)}, u32[]{:S(2)}) copy-start(bf16[8,256,512]{2,1,0:T(8,128)(2,1)} %get-tuple-element.16) | copy-start | bytes 6291460
  141.5 6.9 %collective-permute-start = (f32[2,256]{1,0:T(2,128)S(1)}, f32[2,256]{1,0:T(2,128)S(1)}, u32[]{:S(2)}, u32[]{:S(2)}) collective-permute-start(f32[2,256]{1,0:T(2,128)S(1)} %pad_maximum_fusion.1), channel_id=1, source_target_pairs={{0,1},{1,0},{2,3},{3,2},{4,5},{5,4},{6,7},{7,6},{8,9},{9,8},{10,11... | collective-permute-start | bytes 6152 | tf_op jit(solution)/shard_map/ppermute | solution.py:423
  145.1 3.1 %copy-start.6 = (f32[2,128,512]{2,0,1:T(2,128)S(1)}, f32[2,128,512]{2,0,1:T(2,128)}, u32[]{:S(2)}) copy-start(f32[2,128,512]{2,0,1:T(2,128)} %get-tuple-element.55) | copy-start | bytes 1572868
  145.2 3.3 %copy-start.9 = (f32[512]{0:T(512)S(1)}, f32[512]{0:T(512)}, u32[]{:S(2)}) copy-start(f32[512]{0:T(512)} %param.22) | copy-start | bytes 6148
  151.3 4.2 %collective-permute-start.1 = (bf16[256,2048]{1,0:T(8,128)(2,1)S(1)}, bf16[256,2048]{1,0:T(8,128)(2,1)S(1)}, u32[]{:S(2)}, u32[]{:S(2)}) collective-permute-start(bf16[256,2048]{1,0:T(8,128)(2,1)S(1)} %dynamic-slice_dynamic-update-slice_fusion), channel_id=1, source_target_pairs={{0,1},{1,0},{2,3},{3,2},{4,5},{5,4},{6,7},{7,6},{8,9},{9,8},{10,11... | collective-permute-start | bytes 3145736 | tf_op jit(solution)/shard_map/ppermute | solution.py:423
  155.5 0.7 copy-start.8
  156.2 71.0 %copy-start.3 = (bf16[256,2048]{1,0:T(8,128)(2,1)}, bf16[256,2048]{1,0:T(8,128)(2,1)S(1)}, u32[]{:S(2)}) copy-start(bf16[256,2048]{1,0:T(8,128)(2,1)S(1)} %get-tuple-element.22.middle) | copy-start | bytes 3145732
  237.1 57.5 %copy-start.1 = (f32[31,512]{1,0:T(8,128)S(1)}, f32[31,512]{1,0:T(8,128)}, u32[]{:S(2)}) copy-start(f32[31,512]{1,0:T(8,128)} %param.21) | copy-start | bytes 190468
where the time goes:
time: 295 us
  Pallas kernels  227 us (77%)
  matrix products  28.4 us (10%)
  other arithmetic  27.1 us (9%)
  local copies, waits for them, and re-layouts  11.4 us (4%)
    pallas_call x3, Pallas kernels, call(): pl.pallas_call(kernel, out_shape=[jax.ShapeDtypeStruct(shape, B16) for sh...  227 us
    dot_general x2, matrix products, feed(): return jnp.dot(hidden.astype(b16), down_flat, preferred_element_type=f32)  19.8 us
    unnamed x48, local copies, waits for them, and re-layouts  9.9 us
  transfers between devices with their start and end apart: 2, of which 0 were waited for; matrix products, arithmetic and copies ran while one was open for 4% of the time, Pallas kernels for 0%

commit v1 on v0

v1 whole, which is shorter than its diff:
```python
import jax
import jax.numpy as jnp
from jax import lax
from jax.experimental import pallas as pl
from jax.experimental.pallas import tpu as pltpu
from jax.sharding import PartitionSpec as P

SEQ_LEN = 128


def rms_rows(rows, gain):
    values = rows.astype(jnp.float32)
    scaled = values * lax.rsqrt(jnp.mean(values * values, axis=-1, keepdims=True) + 1e-05)
    return (scaled * gain).astype(jnp.bfloat16)


def causal_conv(signal, taps):
    width = signal.shape[1]
    seqs = signal.reshape(-1, SEQ_LEN, width)
    result = lax.conv_general_dilated(
        seqs,
        taps[:, None, :],
        (1,),
        [(taps.shape[0] - 1, 0)],
        dimension_numbers=("NWC", "WIO", "NWC"),
        feature_group_count=width,
        precision=lax.Precision.HIGHEST,
    )
    return result.reshape(signal.shape)


def on_device(
    tokens,
    first_gain,
    value_weight,
    gate_weight,
    value_scale,
    gate_scale,
    conv_taps,
    chan_gain,
    mixout_weight,
    mixout_scale,
    second_gain,
    up_weight,
    up_scale,
    down_weight,
    down_scale,
):
    normed = rms_rows(tokens, first_gain)
    count = normed.shape[0]
    width = value_weight.shape[1]
    columns = normed
    value_sum = jnp.dot(
        columns,
        lax.all_gather(value_weight.astype(jnp.bfloat16), "fs", axis=0, tiled=True),
        preferred_element_type=jnp.float32,
    )
    gate_sum = jnp.dot(
        columns,
        lax.all_gather(gate_weight.astype(jnp.bfloat16), "fs", axis=0, tiled=True),
        preferred_element_type=jnp.float32,
    )
    value_mult = value_scale.astype(jnp.bfloat16).astype(jnp.float32)
    gate_mult = gate_scale.astype(jnp.bfloat16).astype(jnp.float32)
    glu = value_sum * value_mult * jax.nn.sigmoid(gate_sum * gate_mult)
    conv = causal_conv(glu, conv_taps)
    total = width * lax.axis_size("tp")
    sums, squares = lax.psum((jnp.sum(conv, axis=1), jnp.sum(conv * conv, axis=1)), "tp")
    mean = sums / total
    var = squares / total - mean * mean
    centred = conv - mean[:, None]
    mixed_in = jax.nn.silu(centred * lax.rsqrt(var[:, None] + 1e-05) * chan_gain).astype(
        jnp.bfloat16
    )
    out_whole, out_mult = (
        lax.all_gather(mixout_weight.astype(jnp.bfloat16), "fs", axis=1, tiled=True),
        lax.all_gather(mixout_scale.astype(jnp.bfloat16), "fs", axis=0, tiled=True),
    )
    out_factor = out_mult.astype(jnp.float32)
    mix_term = jnp.dot(mixed_in, out_whole, preferred_element_type=jnp.float32) * out_factor
    mix_sum = lax.psum(mix_term.astype(jnp.bfloat16), "tp").astype(jnp.float32)
    middle = (tokens.astype(jnp.float32) + mix_sum).astype(jnp.bfloat16)
    normed2 = rms_rows(middle, second_gain)
    up_empty = jnp.zeros((count, up_weight.shape[1]), jnp.float32)
    piece = lax.all_gather(up_weight.astype(jnp.bfloat16), "fs", axis=0, tiled=True)
    columns = lax.slice_in_dim(normed2, 0, piece.shape[0], axis=1)
    up_sum = up_empty + jnp.dot(columns, piece, preferred_element_type=jnp.float32)
    up_mult = up_scale.astype(jnp.bfloat16).astype(jnp.float32)
    hidden = jnp.square(jax.nn.relu(up_sum * up_mult)).astype(jnp.bfloat16)
    down_whole, down_mult = (
        lax.all_gather(down_weight.astype(jnp.bfloat16), "fs", axis=1, tiled=True),
        lax.all_gather(down_scale.astype(jnp.bfloat16), "fs", axis=0, tiled=True),
    )
    down_factor = down_mult.astype(jnp.float32)
    down_term = jnp.dot(hidden, down_whole, preferred_element_type=jnp.float32) * down_factor
    down_sum = lax.psum(down_term.astype(jnp.bfloat16), "tp").astype(jnp.float32)
    return (middle.astype(jnp.float32) + down_sum).astype(jnp.bfloat16)


MESH = pl.DeviceIdType.MESH
F32, B16 = jnp.float32, jnp.bfloat16
LANES = 128


def aligned(index, step):
    return pl.ds(pl.multiple_of(index * step, step), step)


def flip(index, mask):
    value = index
    bit = 1
    while bit <= mask:
        if mask & bit:
            value = value + bit * (1 - 2 * ((index // bit) % 2))
        bit *= 2
    return value


def remote(src, dst, send_sem, recv_sem, target):
    return pltpu.make_async_remote_copy(
        src_ref=src,
        dst_ref=dst,
        send_sem=send_sem,
        recv_sem=recv_sem,
        device_id=target,
        device_id_type=MESH,
    )


class Exchange:
    def __init__(self, view, order, target, send, recv):
        self.view, self.order, self.target = view, order, target
        self.send, self.recv = send, recv
        self.stages = []

    def start(self):
        done = self.order[: len(self.stages)]
        mask = self.order[len(self.stages)]
        slots = [0]
        for one in done:
            slots += [s ^ one for s in slots]
        copies = []
        for s in slots:
            copy = remote(
                self.view(s, s), self.view(s, s ^ mask), self.send.at[s ^ mask], self.recv.at[s ^ mask], self.target(mask)
            )
            copy.start()
            copies.append((s ^ mask, copy))
        self.stages.append(copies)

    def land(self, stage):
        for _, copy in self.stages[stage]:
            copy.wait_recv()
        return [slot for slot, _ in self.stages[stage]]

    def close(self):
        for stage in self.stages:
            for _, copy in stage:
                copy.wait_send()


def rms(values, gain):
    scale = lax.rsqrt(jnp.mean(values * values, axis=1, keepdims=True) + 1e-05)
    return (values * scale * gain).astype(B16)


GATHER_ORDERS = ((2, 1, 4), (1, 2, 4), (4, 2, 1), (4, 1, 2))
REDUCE_ORDERS = ((4, 2, 1), (1, 4, 2), (2, 1, 4), (4, 1, 2), (1, 2, 4), (2, 4, 1), (4, 2, 1), (1, 4, 2))


def layer_kernel(
    tokens, first_gain, value_w, gate_w, value_scale, gate_scale, taps, chan_gain, mix_w, mix_scale, second_gain,
    up_w, up_scale, down_w, down_scale, out,
    value_in, gate_in, mix_in, up_in, down_in, x_tok, normed, value_all, gate_all, mix_all, up_cut, down_cut,
    up_all, down_all, padded, conv, row_stats, mixed, product, mix_send, mix_recv, mix_keep, half_send, half_recv,
    middle, ours, theirs, acc, hidden, part_send, part_recv, parts, land_a, land_b, land_c,
    load, tok_s, tok_r, w_s, w_r, m_s, m_r, a_s, a_r, st_s, st_r, mp_s, mp_r, mx_s, mx_r,
    g_s, g_r, gt_s, gt_r, p_s, p_r, r_s, r_r, o_s, o_r,
):
    n = 8
    here, rep, tp = lax.axis_index("fs"), lax.axis_index("rep"), lax.axis_index("tp")
    count, wide = tokens.shape
    half = count // 2
    chans = value_in.shape[1]
    hid = up_cut.shape[2]
    cols = mix_in.shape[1]
    depth = value_in.shape[0]
    seq = SEQ_LEN
    partner = {"tp": 1 - tp}
    across = {"rep": 1 - rep}
    corner = {"rep": 1 - rep, "tp": 1 - tp}

    def plane(mask):
        return {"fs": flip(here, mask)}

    def cube(mask):
        return across if mask == 4 else plane(mask)

    loads = [
        pltpu.make_async_copy(value_w.at[:, aligned(rep, chans)], value_in, load.at[0]),
        pltpu.make_async_copy(gate_w.at[:, aligned(rep, chans)], gate_in, load.at[1]),
        pltpu.make_async_copy(mix_w.at[aligned(rep, chans)], mix_in, load.at[2]),
        pltpu.make_async_copy(up_w.at[:, aligned(rep, 4 * hid)], up_in, load.at[3]),
        pltpu.make_async_copy(down_w.at[aligned(rep, 4 * hid)], down_in, load.at[4]),
    ]
    for copy in loads:
        copy.start()
    barrier = pltpu.get_barrier_semaphore()
    peers = [plane(k) for k in range(1, n)] + [partner, across, corner]
    for peer in peers:
        pl.semaphore_signal(barrier, inc=1, device_id=peer, device_id_type=MESH)
    loads[0].wait()
    value_all[here] = value_in[...].astype(B16)
    loads[1].wait()
    gate_all[here] = gate_in[...].astype(B16)
    pl.semaphore_wait(barrier, len(peers))

    closing = []

    own_rows = aligned(tp, half)
    tok = remote(tokens.at[own_rows], x_tok.at[own_rows], tok_s.at[0], tok_r.at[0], across)
    tok.start()
    closing.append(tok)

    piece = depth // 2

    def rows_of(ref, i):
        return lambda s, _: ref.at[flip(here, s), pl.ds(i * piece, piece)]

    first = [
        Exchange(rows_of(value_all, 0), (4, 2, 1), plane, w_s.at[0], w_r.at[0]),
        Exchange(rows_of(gate_all, 0), (4, 1, 2), plane, w_s.at[1], w_r.at[1]),
        Exchange(rows_of(value_all, 1), (4, 2, 1), plane, w_s.at[2], w_r.at[2]),
        Exchange(rows_of(gate_all, 1), (4, 2, 1), plane, w_s.at[3], w_r.at[3]),
    ]
    for one in first:
        one.start()

    loads[2].wait()
    factor = mix_scale[...].astype(B16).astype(F32)
    mix_all[here] = (mix_in[...].astype(B16).astype(F32) * factor).astype(B16)
    loads[3].wait()
    for j in range(4):
        up_cut[j] = up_in[:, j * hid : (j + 1) * hid].astype(B16)
    own = here % 4
    up_all[here] = up_in[:, aligned(own, hid)].astype(B16)

    sent = []

    def push(*items):
        for kind, s in items:
            to = flip(here, s)
            if kind == "u":
                copy = remote(up_cut.at[to % 4], up_all.at[here], a_s.at[s], a_r.at[s], {"fs": to})
            else:
                copy = remote(down_cut.at[to % 4], down_all.at[here], a_s.at[n + s], a_r.at[n + s], {"fs": to})
            copy.start()
            sent.append((kind, s, copy))

    def arrived(kind, slots):
        for one, s, copy in sent:
            if one == kind and s in slots:
                copy.wait_recv()

    push(("u", 4))

    def norm_block(src, at):
        def body(i, _):
            there = pl.ds(pl.multiple_of(i * 32, 32), 32)
            values = src[there].astype(F32)
            normed[pl.ds(pl.multiple_of(at * count + i * 32, 32), 32)] = rms(values, first_gain[...])
            return 0

        lax.fori_loop(0, count // 32, body, 0)

    norm_block(tokens, rep)
    for one in first:
        one.land(0)
        one.start()
    push(("u", 5))
    loads[4].wait()
    factor_d = down_scale[...].astype(B16).astype(F32)
    for j in range(4):
        block = down_in[j * hid : (j + 1) * hid].astype(B16).astype(F32) * factor_d
        down_cut[j] = block.astype(B16)
    down_all[here] = (down_in[aligned(own, hid)].astype(B16).astype(F32) * factor_d).astype(B16)

    tok.wait_recv()
    tok_on = remote(x_tok.at[own_rows], x_tok.at[own_rows], tok_s.at[1], tok_r.at[1], partner)
    tok_on.start()
    closing.append(tok_on)

    for one in first:
        one.land(1)
        one.start()
    second = [
        Exchange(rows_of(mix_all, 0), (4, 2, 1), plane, m_s.at[0], m_r.at[0]),
        Exchange(rows_of(mix_all, 1), (4, 1, 2), plane, m_s.at[1], m_r.at[1]),
    ]
    for one in second:
        one.start()
    push(("u", 6))
    tok_on.wait_recv()
    norm_block(x_tok, 1 - rep)
    for one in second:
        one.land(0)
        one.start()
    push(("u", 7))
    for one in first:
        one.land(2)
    for one in second:
        one.land(1)
        one.start()
    push(("u", 1), ("u", 2), ("u", 3), ("d", 1), ("d", 2), ("d", 3))

    value_mult = value_scale[:, aligned(rep, chans)].astype(B16).astype(F32)
    gate_mult = gate_scale[:, aligned(rep, chans)].astype(B16).astype(F32)
    wv = value_all[...].reshape(n * depth, chans)
    wg = gate_all[...].reshape(n * depth, chans)
    pad = padded.shape[1] - seq
    for b in range(padded.shape[0]):
        rows = normed[b * seq : (b + 1) * seq]
        value = jnp.dot(rows, wv, preferred_element_type=F32)
        gate = jnp.dot(rows, wg, preferred_element_type=F32)
        padded[b, :pad] = jnp.zeros((pad, chans), F32)
        padded[b, pad:] = value * value_mult * jax.nn.sigmoid(gate * gate_mult)

    n_taps = taps.shape[0]
    eye = lax.broadcasted_iota(jnp.int32, (seq, seq), 0) == lax.broadcasted_iota(jnp.int32, (seq, seq), 1)
    gain = chan_gain[:, aligned(rep, chans)]
    tap_rows = taps[:, aligned(rep, chans)]

    for b in range(padded.shape[0]):
        sums = jnp.zeros((seq, 1), F32)
        squares = jnp.zeros((seq, 1), F32)
        for lane in range(chans // LANES):
            at = slice(lane * LANES, (lane + 1) * LANES)
            total = jnp.zeros((seq, LANES), F32)
            start = pad - n_taps + 1
            for shift in range(8):
                offsets = [o for o in range(start, pad + 1) if o % 8 == shift]
                if not offsets:
                    continue
                low = offsets[0]
                span = offsets[-1] - low + seq
                window = padded[b, low : low + span, at]
                for o in offsets:
                    tap = tap_rows[o - start : o - start + 1, at]
                    total = total + tap * window[o - low : o - low + seq]
            conv[b, :, at] = total
            sums = sums + jnp.sum(total, axis=1, keepdims=True)
            squares = squares + jnp.sum(total * total, axis=1, keepdims=True)
        row_stats[0, b : b + 1] = jnp.sum(jnp.where(eye, sums, 0.0), axis=0, keepdims=True)
        row_stats[0, 4 + b : 5 + b] = jnp.sum(jnp.where(eye, squares, 0.0), axis=0, keepdims=True)

    stats = []
    for i, target in enumerate((partner, across, corner)):
        copy = remote(row_stats.at[0], row_stats.at[1 + i], st_s.at[i], st_r.at[i], target)
        copy.start()
        stats.append(copy)
    for copy in stats:
        copy.wait_recv()
    closing += stats
    both = row_stats[0] + row_stats[1] + row_stats[2] + row_stats[3]
    n_chans = chans * 4
    means = both[:4] / n_chans
    scales = lax.rsqrt(both[4:] / n_chans - means * means + 1e-05)
    for b in range(padded.shape[0]):
        mean = jnp.sum(jnp.where(eye, means[b : b + 1], 0.0), axis=1, keepdims=True)
        scale = jnp.sum(jnp.where(eye, scales[b : b + 1], 0.0), axis=1, keepdims=True)
        level = (conv[b] - mean) * scale * gain
        mixed[b * seq : (b + 1) * seq] = (level / (1.0 + jnp.exp(-level))).astype(B16)

    for one in second:
        one.land(2)

    def kept_rows(r, t):
        return pl.ds(pl.multiple_of(r * count + t * half, half), half)

    passes, hops = [], []
    for f in range(n):
        product[...] = jnp.dot(mixed[...], mix_all[f], preferred_element_type=F32)
        for r in range(2):
            mix_send[f, r] = product[kept_rows(r, 1 - tp)].astype(B16)
            mix_keep[f, r] = product[kept_rows(r, tp)]
        copy = remote(mix_send.at[f], mix_recv.at[f], mp_s.at[f], mp_r.at[f], partner)
        copy.start()
        passes.append(copy)
        if f >= 1:
            fold_pass(f - 1, passes, mix_keep, mix_recv, half_send, half_recv, mx_s, mx_r, across, rep, hops)
    fold_pass(n - 1, passes, mix_keep, mix_recv, half_send, half_recv, mx_s, mx_r, across, rep, hops)
    closing += passes + hops
    norm_sum = jnp.zeros((half, 1), F32)
    for f in range(n):
        at = slice(f * cols, (f + 1) * cols)
        hops[f].wait_recv()
        total = mix_keep[f, rep] + mix_recv[f, rep].astype(F32) + half_recv[f].astype(F32)
        block = (tokens[own_rows, at].astype(F32) + total).astype(B16)
        middle[:, at] = block
        wide_block = block.astype(F32)
        norm_sum = norm_sum + jnp.sum(wide_block * wide_block, axis=1, keepdims=True)
    scale2 = lax.rsqrt(norm_sum / wide + 1e-05)
    chunk = ours.shape[2]
    n_chunks = ours.shape[0]
    for q in range(n_chunks):
        at = slice(q * chunk, (q + 1) * chunk)
        ours[q, :half] = (middle[:, at].astype(F32) * scale2 * second_gain[:, at]).astype(B16)

    def slot_of(ref, q):
        return lambda s, to: ref.at[q, pl.ds(to * half, half)]

    gathers = [
        Exchange(slot_of(ours, q), GATHER_ORDERS[q % 4], cube, g_s.at[q], g_r.at[q]) for q in range(n_chunks)
    ]
    forwards = [[] for _ in gathers]

    def forward(q, slots):
        for s in slots:
            there = pl.ds(s * half, half)
            copy = remote(ours.at[q, there], theirs.at[q, there], gt_s.at[q, s], gt_r.at[q, s], partner)
            copy.start()
            forwards[q].append(copy)

    for one in gathers:
        one.start()
    for q in range(n_chunks):
        forward(q, [0])
    far = [("d", 4), ("d", 5), ("d", 6), ("d", 7)]
    push(*far[:1])
    for q, one in enumerate(gathers):
        slots = one.land(0)
        one.start()
        forward(q, slots)
    push(*far[1:2])
    for q, one in enumerate(gathers):
        slots = one.land(1)
        one.start()
        forward(q, slots)
    push(*far[2:])
    arrived("u", range(1, n))
    rows_all = n * half
    step = 256
    last_mult = up_scale[:, aligned(rep * 4 + own, hid)].astype(B16).astype(F32)
    for q, one in enumerate(gathers):
        forward(q, one.land(2))
        for copy in forwards[q]:
            copy.wait_recv()
        for side, ref in enumerate((ours, theirs)):
            def body(i, _, q=q, side=side, ref=ref):
                there = pl.ds(pl.multiple_of(i * step, step), step)
                into = pl.ds(pl.multiple_of(side * rows_all + i * step, step), step)
                w = up_all[q * (chunk // depth) : (q + 1) * (chunk // depth)].reshape(chunk, hid)
                value = jnp.dot(ref[q, there], w, preferred_element_type=F32)
                if q > 0:
                    value = value + acc[into]
                if q < n_chunks - 1:
                    acc[into] = value
                else:
                    value = jnp.maximum(value * last_mult, 0.0)
                    hidden[into] = (value * value).astype(B16)
                return 0

            lax.fori_loop(0, rows_all // step, body, 0)

    arrived("d", range(1, 4))
    near = here // 4

    def group(g):
        return (g + 4 * near) % n

    lands = (land_a, land_b, land_c)
    passed, flights, finals = [], [[] for _ in range(n)], []

    def multiply(g):
        w = down_all[group(g)]
        for side, ref in ((1, part_send), (0, parts)):
            def body(i, _, side=side, ref=ref):
                there = pl.ds(pl.multiple_of(i * step, step), step)
                from_rows = pl.ds(pl.multiple_of(side * rows_all + i * step, step), step)
                ref[g, there] = jnp.dot(hidden[from_rows], w, preferred_element_type=F32).astype(B16)
                return 0

            lax.fori_loop(0, rows_all // step, body, 0)
            if side == 1:
                copy = remote(part_send.at[g], part_recv.at[g], p_s.at[g], p_r.at[g], partner)
                copy.start()
                passed.append(copy)

    def rows(s):
        return slice(s * half, (s + 1) * half)

    def going(g, stage):
        order = REDUCE_ORDERS[g]
        kept = [s for s in range(n) if not any(s & m for m in order[:stage])]
        mask = order[stage]
        return [s for s in kept if s & mask], [s for s in kept if not s & mask], mask

    def ship(g, stage):
        leave, _, mask = going(g, stage)
        for i, s in enumerate(leave):
            sem = (0, 4, 6)[stage] + i
            copy = remote(
                parts.at[g, pl.ds(s * half, half)],
                lands[stage].at[g, pl.ds(i * half, half)],
                r_s.at[g, sem],
                r_r.at[g, sem],
                cube(mask),
            )
            copy.start()
            flights[g].append((stage, i, s ^ mask, copy))

    def begin(g):
        passed[g].wait_recv()
        leave, stay, _ = going(g, 0)
        for s in leave:
            there = rows(s)
            parts[g, there] = (parts[g, there].astype(F32) + part_recv[g, there].astype(F32)).astype(B16)
        ship(g, 0)

    def advance(g, stage):
        came = [(i, s) for at, i, s, copy in flights[g] if at == stage]
        for at, i, s, copy in flights[g]:
            if at == stage:
                copy.wait_recv()
        for i, s in came:
            there = rows(s)
            value = parts[g, there].astype(F32) + lands[stage][g, rows(i)].astype(F32)
            if stage == 0:
                value = value + part_recv[g, there].astype(F32)
            if stage < 2:
                parts[g, there] = value.astype(B16)
            else:
                at = aligned(group(g), cols)
                out[own_rows, at] = (middle[:, at].astype(F32) + value).astype(B16)
        if stage < 2:
            ship(g, stage + 1)
        else:
            at = aligned(group(g), cols)
            copy = remote(out.at[own_rows, at], out.at[own_rows, at], o_s.at[g], o_r.at[g], partner)
            copy.start()
            finals.append(copy)

    events = []
    for g in range(n):
        events += [(g, 0, g), (g + 1, 1, g), (g + 3, 2, g), (g + 5, 3, g), (g + 7, 4, g)]
    for _, kind, g in sorted(events, key=lambda e: (e[0], -e[1])):
        if kind == 0:
            if g == 4:
                arrived("d", range(4, n))
            multiply(g)
        elif kind == 1:
            begin(g)
        else:
            advance(g, kind - 2)

    for one in first + second + gathers:
        one.close()
    for some in forwards + [[c for _, _, c in sent], closing, passed, finals]:
        for copy in some:
            copy.wait_send()
    for some in flights:
        for _, _, _, copy in some:
            copy.wait_send()
    for copy in finals:
        copy.wait_recv()


def fold_pass(f, passes, mix_keep, mix_recv, half_send, half_recv, mx_s, mx_r, across, rep, hops):
    passes[f].wait_recv()
    half_send[f] = (mix_keep[f, 1 - rep] + mix_recv[f, 1 - rep].astype(F32)).astype(B16)
    copy = remote(half_send.at[f], half_recv.at[f], mx_s.at[f], mx_r.at[f], across)
    copy.start()
    hops.append(copy)


def layer_device(
    tokens, first_gain, value_weight, gate_weight, value_scale, gate_scale, conv_taps, chan_gain, mixout_weight,
    mixout_scale, second_gain, up_weight, up_scale, down_weight, down_scale,
):
    n = 8
    count, wide = tokens.shape
    depth, chans = value_weight.shape[0], value_weight.shape[1] // 2
    hid = up_weight.shape[1] // n
    cols = mixout_weight.shape[1]
    half = count // 2
    chunk = wide // 4
    rows = n * half
    vm, anywhere = pl.BlockSpec(memory_space=pltpu.VMEM), pl.BlockSpec(memory_space=pl.ANY)
    dma = pltpu.SemaphoreType.DMA

    def line(values):
        return values.reshape(1, -1)

    operands = [
        (tokens, vm),
        (line(first_gain), vm),
        (value_weight, anywhere),
        (gate_weight, anywhere),
        (line(value_scale), vm),
        (line(gate_scale), vm),
        (conv_taps, vm),
        (line(chan_gain), vm),
        (mixout_weight, anywhere),
        (line(mixout_scale), vm),
        (line(second_gain), vm),
        (up_weight, anywhere),
        (line(up_scale), vm),
        (down_weight, anywhere),
        (line(down_scale), vm),
    ]
    seqs = 2 * count // SEQ_LEN
    scratch = [
        ((depth, chans), F32),
        ((depth, chans), F32),
        ((chans, cols), F32),
        ((depth, 4 * hid), F32),
        ((4 * hid, cols), F32),
        ((count, wide), B16),
        ((2 * count, wide), B16),
        ((n, depth, chans), B16),
        ((n, depth, chans), B16),
        ((n, chans, cols), B16),
        ((4, depth, hid), B16),
        ((4, hid, cols), B16),
        ((n, depth, hid), B16),
        ((n, hid, cols), B16),
        ((seqs, SEQ_LEN + 32, chans), F32),
        ((seqs, SEQ_LEN, chans), F32),
        ((4, 8, SEQ_LEN), F32),
        ((2 * count, chans), B16),
        ((2 * count, cols), F32),
        ((n, 2, half, cols), B16),
        ((n, 2, half, cols), B16),
        ((n, 2, half, cols), F32),
        ((n, half, cols), B16),
        ((n, half, cols), B16),
        ((half, wide), B16),
        ((4, rows, chunk), B16),
        ((4, rows, chunk), B16),
        ((2 * rows, hid), F32),
        ((2 * rows, hid), B16),
        ((n, rows, cols), B16),
        ((n, rows, cols), B16),
        ((n, rows, cols), B16),
        ((n, 4 * half, cols), B16),
        ((n, 2 * half, cols), B16),
        ((n, half, cols), B16),
    ]
    sems = [(5,), (2,), (2,), (4, n), (4, n), (2, n), (2, n), (2 * n,), (2 * n,), (3,), (3,), (n,), (n,), (n,), (n,)]
    sems += [(4, n), (4, n), (4, n), (4, n), (n,), (n,), (n, n), (n, n), (n,), (n,)]
    return pl.pallas_call(
        layer_kernel,
        out_shape=jax.ShapeDtypeStruct((count, wide), B16),
        in_specs=[spec for _, spec in operands],
        out_specs=vm,
        scratch_shapes=[pltpu.VMEM(shape, kind) for shape, kind in scratch] + [dma(shape) for shape in sems],
        compiler_params=pltpu.CompilerParams(
            collective_id=0, has_side_effects=True, vmem_limit_bytes=60 * 1024 * 1024
        ),
    )(*[array for array, _ in operands])


def solution(mesh):
    placed = (
        P(("rep", "fs"), None),
        P(),
        P("fs", "tp"),
        P("fs", "tp"),
        P("tp"),
        P("tp"),
        P(None, "tp"),
        P("tp"),
        P("tp", "fs"),
        P("fs"),
        P(),
        P("fs", "tp"),
        P("tp"),
        P("tp", "fs"),
        P("fs"),
    )
    fits = mesh.shape["rep"] == 2 and mesh.shape["tp"] == 2 and mesh.shape["fs"] == 8
    return jax.shard_map(
        layer_device if fits else on_device,
        mesh=mesh,
        in_specs=placed,
        out_specs=P(("rep", "fs"), None),
        check_vma=False,
    )
```

time: 295 us -> 197 us (0.67)
  Pallas kernels: 227 us -> 194 us
  matrix products: 28.4 us -> 0 us
  other arithmetic: 27.1 us -> 0 us
  local copies, waits for them, and re-layouts: 11.4 us -> 2.3 us
    pallas_call x3 -> x1, Pallas kernels: 227 us -> 194 us  [layer_device(): pl.pallas_call(layer_kernel, out_shape=jax.ShapeDtypeStruct((count, wide)...]
    dot_general x5 -> x0, matrix products: 25.4 us -> none  [the longest x2 19.8 us: feed(): return jnp.dot(hidden.astype(b16), down_flat, preferred_element_type=f32)]
    convert_element_type x10 -> x0, other arithmetic: 11.3 us -> none  [the longest x1 3.45 us: ring_device(): own_cut = jnp.where(first_rep, up_cut, down_cut).astype(b16)]
    unnamed x48 -> x1, local copies, waits for them, and re-layouts: 9.9 us -> 2.3 us
    unnamed x7 -> x0, other arithmetic: 5.25 us -> none
    select_n x1 -> x0, other arithmetic: 3.21 us -> none  [ring_device(): up_flat = jnp.where(first_rep, own_flat, rest_flat).reshape(n * depth, wide)]
    conv_general_dilated x1 -> x0, matrix products: 3.02 us -> none  [causal_conv(): lax.conv_general_dilated(seqs, taps[:, None, :], (1,), [(taps.shape[0] -...]
  transfers between devices with their start and end apart: 2 -> 0, of which waited for: 0 -> 0; matrix products, arithmetic and copies ran while one was open for 4% -> 0% of each run, Pallas kernels for 0% -> 0%
where the time goes in v1:
time: 197 us; the launch traced here: 196 us
  Pallas kernels  194 us (98%)
  local copies, waits for them, and re-layouts  2.3 us (1%)
    pallas_call x1, Pallas kernels, layer_device(): pl.pallas_call(layer_kernel, out_shape=jax.ShapeDtypeStruct((count, wide)...  194 us

profile of v1, /device:TPU:0, one launch (start us, length us, event | category | flops | bytes accessed | tf_op | source)
XLA Modules:
  0.0 196.4 jit_solution(8283140488299512325)
XLA Ops:
  0.0 194.1 %shard_map.145 = bf16[256,2048]{1,0:T(8,128)(2,1)} custom-call(bf16[256,2048]{1,0:T(8,128)(2,1)} %tokens.1, f32[1,2048]{1,0:T(1,128)} %bitcast.9, f32[256,512]{1,0:T(8,128)} %value_w.1, f32[256,512]{1,0:T(8,128)} %gate_w.1, f32[1,512]{1,0:T(1,128)} %bitcast.11, f32[1,512]{1,0:T(1,128)} %bitcast.12, f32[31,512]{1,0:T(8,128)} %taps.1, f32[1,512]{1,0:T(1,128)} %bitcast.13, ...), custom_call_target="tpu_custom_call" | custom-call | tf_op jit(solution)/shard_map/pallas_call | solution.py:651
  194.1 2.3 %copy.17 = bf16[256,2048]{1,0:T(8,128)(2,1)} copy(bf16[256,2048]{1,0:T(8,128)(2,1)} %shard_map.145) | data formatting | bytes 2097152

commit v2 on v1

--- a/solution.py
+++ b/solution.py
@@ -164,8 +164,14 @@
     return (values * scale * gain).astype(B16)
 
 
+INNER = {'u': (0, 8, 8, 8, 1, 2, 4, 13), 'd': (0, 14, 15, 16, 31, 35, 38, 38)}
+OUTER = {'u': (0, 8, 8, 8, 1, 2, 24, 13), 'd': (0, 14, 15, 16, 35, 36, 38, 38)}
+SECOND_AT = (2, 4, 8)
+FIRST_ORDERS = ((4, 2, 1), (4, 1, 2), (4, 2, 1), (4, 2, 1))
+SECOND_ORDERS = ((4, 2, 1), (4, 1, 2))
 GATHER_ORDERS = ((2, 1, 4), (1, 2, 4), (4, 2, 1), (4, 1, 2))
-REDUCE_ORDERS = ((4, 2, 1), (1, 4, 2), (2, 1, 4), (4, 1, 2), (1, 2, 4), (2, 4, 1), (4, 2, 1), (1, 4, 2))
+REDUCE_ORDERS = ((4, 2, 1), (1, 4, 2), (4, 1, 2), (2, 1, 4), (1, 2, 4), (4, 1, 2), (2, 4, 1), (1, 2, 4))
+TIMES = ((0.0, 1.5), (3.0, 1.5), (11.0, 1.75), (16.0, 1.9), (23.0, 1.8))
 
 
 def layer_kernel(
@@ -173,7 +179,7 @@
     up_w, up_scale, down_w, down_scale, out,
     value_in, gate_in, mix_in, up_in, down_in, x_tok, normed, value_all, gate_all, mix_all, up_cut, down_cut,
     up_all, down_all, padded, conv, row_stats, mixed, product, mix_send, mix_recv, mix_keep, half_send, half_recv,
-    middle, ours, theirs, acc, hidden, part_send, part_recv, parts, land_a, land_b, land_c,
+    middle, ours, theirs, acc, hidden, part_recv, land_a, land_b, land_c,
     load, tok_s, tok_r, w_s, w_r, m_s, m_r, a_s, a_r, st_s, st_r, mp_s, mp_r, mx_s, mx_r,
     g_s, g_r, gt_s, gt_r, p_s, p_r, r_s, r_r, o_s, o_r,
 ):
@@ -228,10 +234,10 @@
         return lambda s, _: ref.at[flip(here, s), pl.ds(i * piece, piece)]
 
     first = [
-        Exchange(rows_of(value_all, 0), (4, 2, 1), plane, w_s.at[0], w_r.at[0]),
-        Exchange(rows_of(gate_all, 0), (4, 1, 2), plane, w_s.at[1], w_r.at[1]),
-        Exchange(rows_of(value_all, 1), (4, 2, 1), plane, w_s.at[2], w_r.at[2]),
-        Exchange(rows_of(gate_all, 1), (4, 2, 1), plane, w_s.at[3], w_r.at[3]),
+        Exchange(rows_of(value_all, 0), FIRST_ORDERS[0], plane, w_s.at[0], w_r.at[0]),
+        Exchange(rows_of(gate_all, 0), FIRST_ORDERS[1], plane, w_s.at[1], w_r.at[1]),
+        Exchange(rows_of(value_all, 1), FIRST_ORDERS[2], plane, w_s.at[2], w_r.at[2]),
+        Exchange(rows_of(gate_all, 1), FIRST_ORDERS[3], plane, w_s.at[3], w_r.at[3]),
     ]
     for one in first:
         one.start()
@@ -245,24 +251,44 @@
     own = here % 4
     up_all[here] = up_in[:, aligned(own, hid)].astype(B16)
 
-    sent = []
-
-    def push(*items):
-        for kind, s in items:
-            to = flip(here, s)
-            if kind == "u":
-                copy = remote(up_cut.at[to % 4], up_all.at[here], a_s.at[s], a_r.at[s], {"fs": to})
-            else:
-                copy = remote(down_cut.at[to % 4], down_all.at[here], a_s.at[n + s], a_r.at[n + s], {"fs": to})
-            copy.start()
-            sent.append((kind, s, copy))
+    def block_copy(kind, s):
+        to = flip(here, s)
+        if kind == "u":
+            return remote(up_cut.at[to % 4], up_all.at[here], a_s.at[s], a_r.at[s], {"fs": to})
+        return remote(down_cut.at[to % 4], down_all.at[here], a_s.at[n + s], a_r.at[n + s], {"fs": to})
+
+    layer = here // 2
+    inner = jnp.logical_and(layer > 0, layer < 3)
+
+    point = [0]
+
+    def push():
+        at = point[0]
+        point[0] += 1
+        mine = [(kind, s) for kind in "ud" for s in range(1, n) if INNER[kind][s] == at]
+        theirs = [(kind, s) for kind in "ud" for s in range(1, n) if OUTER[kind][s] == at]
+        always = [one for one in mine if one in theirs]
+        for one in always:
+            block_copy(*one).start()
+        for side, items in ((inner, mine), (jnp.logical_not(inner), theirs)):
+            items = [one for one in items if one not in always]
+            if items:
+                @pl.when(side)
+                def _(items=items):
+                    for one in items:
+                        block_copy(*one).start()
+        if at == SECOND_AT[0]:
+            for one in second:
+                one.start()
+        for stage in range(2):
+            if at == SECOND_AT[stage + 1]:
+                for one in second:
+                    one.land(stage)
+                    one.start()
 
     def arrived(kind, slots):
-        for one, s, copy in sent:
-            if one == kind and s in slots:
-                copy.wait_recv()
-
-    push(("u", 4))
+        for s in slots:
+            block_copy(kind, s).wait_recv()
 
     def norm_block(src, at):
         def body(i, _):
@@ -273,45 +299,37 @@
 
         lax.fori_loop(0, count // 32, body, 0)
 
-    norm_block(tokens, rep)
-    for one in first:
-        one.land(0)
-        one.start()
-    push(("u", 5))
+    second = [
+        Exchange(rows_of(mix_all, 0), SECOND_ORDERS[0], plane, m_s.at[0], m_r.at[0]),
+        Exchange(rows_of(mix_all, 1), SECOND_ORDERS[1], plane, m_s.at[1], m_r.at[1]),
+    ]
+    push()
     loads[4].wait()
     factor_d = down_scale[...].astype(B16).astype(F32)
     for j in range(4):
         block = down_in[j * hid : (j + 1) * hid].astype(B16).astype(F32) * factor_d
         down_cut[j] = block.astype(B16)
     down_all[here] = (down_in[aligned(own, hid)].astype(B16).astype(F32) * factor_d).astype(B16)
+    norm_block(tokens, rep)
+    for one in first:
+        one.land(0)
+        one.start()
+    push()
 
     tok.wait_recv()
     tok_on = remote(x_tok.at[own_rows], x_tok.at[own_rows], tok_s.at[1], tok_r.at[1], partner)
     tok_on.start()
     closing.append(tok_on)
-
     for one in first:
         one.land(1)
         one.start()
-    second = [
-        Exchange(rows_of(mix_all, 0), (4, 2, 1), plane, m_s.at[0], m_r.at[0]),
-        Exchange(rows_of(mix_all, 1), (4, 1, 2), plane, m_s.at[1], m_r.at[1]),
-    ]
-    for one in second:
-        one.start()
-    push(("u", 6))
+    push()
     tok_on.wait_recv()
     norm_block(x_tok, 1 - rep)
-    for one in second:
-        one.land(0)
-        one.start()
-    push(("u", 7))
+    push()
     for one in first:
         one.land(2)
-    for one in second:
-        one.land(1)
-        one.start()
-    push(("u", 1), ("u", 2), ("u", 3), ("d", 1), ("d", 2), ("d", 3))
+    push()
 
     value_mult = value_scale[:, aligned(rep, chans)].astype(B16).astype(F32)
     gate_mult = gate_scale[:, aligned(rep, chans)].astype(B16).astype(F32)
@@ -324,6 +342,7 @@
         gate = jnp.dot(rows, wg, preferred_element_type=F32)
         padded[b, :pad] = jnp.zeros((pad, chans), F32)
         padded[b, pad:] = value * value_mult * jax.nn.sigmoid(gate * gate_mult)
+        push()
 
     n_taps = taps.shape[0]
     eye = lax.broadcasted_iota(jnp.int32, (seq, seq), 0) == lax.broadcasted_iota(jnp.int32, (seq, seq), 1)
@@ -352,6 +371,7 @@
             squares = squares + jnp.sum(total * total, axis=1, keepdims=True)
         row_stats[0, b : b + 1] = jnp.sum(jnp.where(eye, sums, 0.0), axis=0, keepdims=True)
         row_stats[0, 4 + b : 5 + b] = jnp.sum(jnp.where(eye, squares, 0.0), axis=0, keepdims=True)
+        push()
 
     stats = []
     for i, target in enumerate((partner, across, corner)):
@@ -360,6 +380,7 @@
         stats.append(copy)
     for copy in stats:
         copy.wait_recv()
+    push()
     closing += stats
     both = row_stats[0] + row_stats[1] + row_stats[2] + row_stats[3]
     n_chans = chans * 4
@@ -386,6 +407,7 @@
         copy = remote(mix_send.at[f], mix_recv.at[f], mp_s.at[f], mp_r.at[f], partner)
         copy.start()
         passes.append(copy)
+        push()
         if f >= 1:
             fold_pass(f - 1, passes, mix_keep, mix_recv, half_send, half_recv, mx_s, mx_r, across, rep, hops)
     fold_pass(n - 1, passes, mix_keep, mix_recv, half_send, half_recv, mx_s, mx_r, across, rep, hops)
@@ -399,6 +421,7 @@
         middle[:, at] = block
         wide_block = block.astype(F32)
         norm_sum = norm_sum + jnp.sum(wide_block * wide_block, axis=1, keepdims=True)
+        push()
     scale2 = lax.rsqrt(norm_sum / wide + 1e-05)
     chunk = ours.shape[2]
     n_chunks = ours.shape[0]
@@ -425,26 +448,26 @@
         one.start()
     for q in range(n_chunks):
         forward(q, [0])
-    far = [("d", 4), ("d", 5), ("d", 6), ("d", 7)]
-    push(*far[:1])
+    push()
     for q, one in enumerate(gathers):
         slots = one.land(0)
         one.start()
         forward(q, slots)
-    push(*far[1:2])
+        push()
     for q, one in enumerate(gathers):
         slots = one.land(1)
         one.start()
         forward(q, slots)
-    push(*far[2:])
+        push()
     arrived("u", range(1, n))
     rows_all = n * half
-    step = 256
+    step = 1024
     last_mult = up_scale[:, aligned(rep * 4 + own, hid)].astype(B16).astype(F32)
     for q, one in enumerate(gathers):
         forward(q, one.land(2))
         for copy in forwards[q]:
             copy.wait_recv()
+        push()
         for side, ref in enumerate((ours, theirs)):
             def body(i, _, q=q, side=side, ref=ref):
                 there = pl.ds(pl.multiple_of(i * step, step), step)
@@ -471,23 +494,33 @@
     lands = (land_a, land_b, land_c)
     passed, flights, finals = [], [[] for _ in range(n)], []
 
+    for one in gathers:
+        one.close()
+    for some in forwards:
+        for copy in some:
+            copy.wait_send()
+    per = chunk // cols
+
+    def block_at(ref, g, there):
+        return ref.at[g // per, there, pl.ds((g % per) * cols, cols)]
+
     def multiply(g):
         w = down_all[group(g)]
-        for side, ref in ((1, part_send), (0, parts)):
+        for side, ref in ((1, theirs), (0, ours)):
             def body(i, _, side=side, ref=ref):
                 there = pl.ds(pl.multiple_of(i * step, step), step)
                 from_rows = pl.ds(pl.multiple_of(side * rows_all + i * step, step), step)
-                ref[g, there] = jnp.dot(hidden[from_rows], w, preferred_element_type=F32).astype(B16)
+                block_at(ref, g, there)[...] = jnp.dot(hidden[from_rows], w, preferred_element_type=F32).astype(B16)
                 return 0
 
             lax.fori_loop(0, rows_all // step, body, 0)
             if side == 1:
-                copy = remote(part_send.at[g], part_recv.at[g], p_s.at[g], p_r.at[g], partner)
+                copy = remote(block_at(theirs, g, pl.ds(0, rows_all)), part_recv.at[g], p_s.at[g], p_r.at[g], partner)
                 copy.start()
                 passed.append(copy)
 
     def rows(s):
-        return slice(s * half, (s + 1) * half)
+        return pl.ds(s * half, half)
 
     def going(g, stage):
         order = REDUCE_ORDERS[g]
@@ -500,7 +533,7 @@
         for i, s in enumerate(leave):
             sem = (0, 4, 6)[stage] + i
             copy = remote(
-                parts.at[g, pl.ds(s * half, half)],
+                block_at(ours, g, pl.ds(s * half, half)),
                 lands[stage].at[g, pl.ds(i * half, half)],
                 r_s.at[g, sem],
                 r_r.at[g, sem],
@@ -514,7 +547,8 @@
         leave, stay, _ = going(g, 0)
         for s in leave:
             there = rows(s)
-            parts[g, there] = (parts[g, there].astype(F32) + part_recv[g, there].astype(F32)).astype(B16)
+            part = block_at(ours, g, there)
+            part[...] = (part[...].astype(F32) + part_recv[g, there].astype(F32)).astype(B16)
         ship(g, 0)
 
     def advance(g, stage):
@@ -524,11 +558,12 @@
                 copy.wait_recv()
         for i, s in came:
             there = rows(s)
-            value = parts[g, there].astype(F32) + lands[stage][g, rows(i)].astype(F32)
+            part = block_at(ours, g, there)
+            value = part[...].astype(F32) + lands[stage][g, rows(i)].astype(F32)
             if stage == 0:
                 value = value + part_recv[g, there].astype(F32)
             if stage < 2:
-                parts[g, there] = value.astype(B16)
+                part[...] = value.astype(B16)
             else:
                 at = aligned(group(g), cols)
                 out[own_rows, at] = (middle[:, at].astype(F32) + value).astype(B16)
@@ -540,22 +575,25 @@
             copy.start()
             finals.append(copy)
 
-    events = []
-    for g in range(n):
-        events += [(g, 0, g), (g + 1, 1, g), (g + 3, 2, g), (g + 5, 3, g), (g + 7, 4, g)]
-    for _, kind, g in sorted(events, key=lambda e: (e[0], -e[1])):
+    events = [(at + pace * g, -kind, g) for kind, (at, pace) in enumerate(TIMES) for g in range(n)]
+    for _, kind, g in sorted(events):
+        kind = -kind
         if kind == 0:
             if g == 4:
                 arrived("d", range(4, n))
             multiply(g)
+            push()
         elif kind == 1:
             begin(g)
         else:
             advance(g, kind - 2)
 
-    for one in first + second + gathers:
+    for one in first + second:
         one.close()
-    for some in forwards + [[c for _, _, c in sent], closing, passed, finals]:
+    for kind in "ud":
+        for s in range(1, n):
+            block_copy(kind, s).wait_send()
+    for some in [closing, passed, finals]:
         for copy in some:
             copy.wait_send()
     for some in flights:
@@ -640,8 +678,6 @@
         ((2 * rows, hid), F32),
         ((2 * rows, hid), B16),
         ((n, rows, cols), B16),
-        ((n, rows, cols), B16),
-        ((n, rows, cols), B16),
         ((n, 4 * half, cols), B16),
         ((n, 2 * half, cols), B16),
         ((n, half, cols), B16),
@@ -655,7 +691,7 @@
         out_specs=vm,
         scratch_shapes=[pltpu.VMEM(shape, kind) for shape, kind in scratch] + [dma(shape) for shape in sems],
         compiler_params=pltpu.CompilerParams(
-            collective_id=0, has_side_effects=True, vmem_limit_bytes=60 * 1024 * 1024
+            collective_id=0, has_side_effects=True, vmem_limit_bytes=63 * 1024 * 1024
         ),
     )(*[array for array, _ in operands])
 

time: 197 us -> 186 us (0.944)
  Pallas kernels: 194 us -> 184 us
    pallas_call x1, Pallas kernels: 194 us -> 184 us  [layer_device(): pl.pallas_call(layer_kernel, out_shape=jax.ShapeDtypeStruct((count, wide)...]
where the time goes in v2:
time: 186 us
  Pallas kernels  184 us (99%)
  local copies, waits for them, and re-layouts  2.3 us (1%)
    pallas_call x1, Pallas kernels, layer_device(): pl.pallas_call(layer_kernel, out_shape=jax.ShapeDtypeStruct((count, wide)...  184 us

profile of v2, /device:TPU:0, one launch (start us, length us, event | category | flops | bytes accessed | tf_op | source)
XLA Modules:
  0.0 186.3 jit_solution(17792558475648350972)
XLA Ops:
  0.0 184.0 %shard_map.145 = bf16[256,2048]{1,0:T(8,128)(2,1)} custom-call(bf16[256,2048]{1,0:T(8,128)(2,1)} %tokens.1, f32[1,2048]{1,0:T(1,128)} %bitcast.9, f32[256,512]{1,0:T(8,128)} %value_w.1, f32[256,512]{1,0:T(8,128)} %gate_w.1, f32[1,512]{1,0:T(1,128)} %bitcast.11, f32[1,512]{1,0:T(1,128)} %bitcast.12, f32[31,512]{1,0:T(8,128)} %taps.1, f32[1,512]{1,0:T(1,128)} %bitcast.13, ...), custom_call_target="tpu_custom_call" | custom-call | tf_op jit(solution)/shard_map/pallas_call | solution.py:687
  184.0 2.3 %copy.17 = bf16[256,2048]{1,0:T(8,128)(2,1)} copy(bf16[256,2048]{1,0:T(8,128)(2,1)} %shard_map.145) | data formatting | bytes 2097152

commit v3 on v2

--- a/solution.py
+++ b/solution.py
@@ -166,7 +166,7 @@
 
 INNER = {'u': (0, 8, 8, 8, 1, 2, 4, 13), 'd': (0, 14, 15, 16, 31, 35, 38, 38)}
 OUTER = {'u': (0, 8, 8, 8, 1, 2, 24, 13), 'd': (0, 14, 15, 16, 35, 36, 38, 38)}
-SECOND_AT = (2, 4, 8)
+SECOND_AT = (2, 4, 6)
 FIRST_ORDERS = ((4, 2, 1), (4, 1, 2), (4, 2, 1), (4, 2, 1))
 SECOND_ORDERS = ((4, 2, 1), (4, 1, 2))
 GATHER_ORDERS = ((2, 1, 4), (1, 2, 4), (4, 2, 1), (4, 1, 2))

time: 186 us -> 183 us (0.984)
  Pallas kernels: 184 us -> 180 us
    pallas_call x1, Pallas kernels: 184 us -> 180 us  [layer_device(): pl.pallas_call(layer_kernel, out_shape=jax.ShapeDtypeStruct((count, wide)...]
where the time goes in v3:
time: 183 us
  Pallas kernels  180 us (98%)
  local copies, waits for them, and re-layouts  2.3 us (1%)
    pallas_call x1, Pallas kernels, layer_device(): pl.pallas_call(layer_kernel, out_shape=jax.ShapeDtypeStruct((count, wide)...  180 us

profile of v3, /device:TPU:0, one launch (start us, length us, event | category | flops | bytes accessed | tf_op | source)
XLA Modules:
  0.0 182.5 jit_solution(9373325341547432520)
XLA Ops:
  0.0 180.2 %shard_map.145 = bf16[256,2048]{1,0:T(8,128)(2,1)} custom-call(bf16[256,2048]{1,0:T(8,128)(2,1)} %tokens.1, f32[1,2048]{1,0:T(1,128)} %bitcast.9, f32[256,512]{1,0:T(8,128)} %value_w.1, f32[256,512]{1,0:T(8,128)} %gate_w.1, f32[1,512]{1,0:T(1,128)} %bitcast.11, f32[1,512]{1,0:T(1,128)} %bitcast.12, f32[31,512]{1,0:T(8,128)} %taps.1, f32[1,512]{1,0:T(1,128)} %bitcast.13, ...), custom_call_target="tpu_custom_call" | custom-call | tf_op jit(solution)/shard_map/pallas_call | solution.py:687
  180.2 2.3 %copy.17 = bf16[256,2048]{1,0:T(8,128)(2,1)} copy(bf16[256,2048]{1,0:T(8,128)(2,1)} %shard_map.145) | data formatting | bytes 2097152
